TPU v7x, 32 devices: a whole 2x2x4 slice. The times are simulated.
32 devices in a mesh: kv: 16 (over z, y, x), tp: 2 (over core).
Axes of the slice: x: 2, y: 2, z: 4, core: 2. Of those that a mesh axis runs over, the one named last changes fastest.
Arguments:
- tokens: bfloat16 [256, 2048], P('kv', 'tp'), may hold values from -20 to 20
- norm_gain: float32 [2048], replicated, may hold values from 0.1 to 1.9
- w_query: bfloat16 [2048, 1024], P(None, 'tp'), may hold values from -0.125 to 0.125
- w_key: bfloat16 [2048, 1024], P(None, 'tp'), may hold values from -0.125 to 0.125
- w_value: bfloat16 [2048, 1024], P(None, 'tp'), may hold values from -0.125 to 0.125
- w_outgate: bfloat16 [2048, 1024], P(None, 'tp'), may hold values from -0.125 to 0.125
- w_input_gate: bfloat16 [2048, 8], replicated, may hold values from -0.125 to 0.125
- w_forget_gate: bfloat16 [2048, 8], replicated, may hold values from -0.125 to 0.125
- memory: float32 [256, 8, 128, 128], P('kv', 'tp'), may hold values from -6 to 6
- normalizer: float32 [256, 8, 128], P('kv', 'tp'), may hold values from -6 to 6
- memory_max: float32 [256, 8], P('kv', 'tp'), may hold values from -2 to 300
- w_output: bfloat16 [1024, 2048], P(None, 'tp'), may hold values from -0.1875 to 0.1875
- ffn_gain: float32 [2048], P('tp'), may hold values from 0.1 to 1.9
- w_gate: bfloat16 [2048, 5632], P('tp', 'kv'), may hold values from -0.125 to 0.125
- w_up: bfloat16 [2048, 5632], P('tp', 'kv'), may hold values from -0.125 to 0.125
- w_down: bfloat16 [5632, 2048], P('kv', 'tp'), may hold values from -0.078125 to 0.078125
Outputs:
- result: bfloat16 [256, 2048], P('kv', 'tp')
- new_memory: float32 [256, 8, 128, 128], P('kv', 'tp')
- new_normalizer: float32 [256, 8, 128], P('kv', 'tp')
- new_max: float32 [256, 8], P('kv', 'tp')
All inputs are finite; a program needn't handle non-finite values.
Results may differ from a plain program's by a relative error of at most 0.013.
Values may be sent and summed in bfloat16 or wider, within the bound.
A program may use at most 64 MiB of HBM per device.

v0:
```python
import jax
import jax.numpy as jnp
from jax import lax
from jax.sharding import PartitionSpec as P

D = 2048


def activate(gate_sum, up_sum, square_sum):
    ffn_scale = lax.rsqrt(square_sum / D + 1e-06)[:, None]
    return (jax.nn.silu(ffn_scale * gate_sum) * (ffn_scale * up_sum)).astype(jnp.bfloat16)


def per_device(
    tokens,
    norm_gain,
    w_query,
    w_key,
    w_value,
    w_outgate,
    w_input_gate,
    w_forget_gate,
    memory,
    normalizer,
    memory_max,
    w_output,
    ffn_gain,
    w_gate,
    w_up,
    w_down,
):
    local_rows = tokens.shape[0]
    head_count = memory.shape[1]
    head_dim = memory.shape[2]
    full_rows = lax.all_gather(tokens, "tp", axis=1, tiled=True)
    rows_f = full_rows.astype(jnp.float32)
    row_scale = lax.rsqrt(jnp.mean(rows_f * rows_f, axis=-1, keepdims=True) + 1e-06)
    normed = (rows_f * row_scale * norm_gain).astype(jnp.bfloat16)

    def project(weight):
        return jnp.dot(normed, weight, preferred_element_type=jnp.float32).reshape(
            local_rows, head_count, head_dim
        )

    queries = project(w_query) * head_dim ** (-0.5)
    key_vec = project(w_key)
    values = project(w_value)
    outgate = project(w_outgate)
    first_head = lax.axis_index("tp") * head_count
    igate = lax.dynamic_slice_in_dim(
        jnp.dot(normed, w_input_gate, preferred_element_type=jnp.float32), first_head, head_count, 1
    )
    forget_pre = lax.dynamic_slice_in_dim(
        jnp.dot(normed, w_forget_gate, preferred_element_type=jnp.float32),
        first_head,
        head_count,
        1,
    )
    lforget = jax.nn.log_sigmoid(forget_pre)
    new_max = jnp.maximum(lforget + memory_max, igate)
    keep_weight = jnp.exp(lforget + memory_max - new_max)
    admit_weight = jnp.exp(igate - new_max)
    new_memory = keep_weight[..., None, None] * memory + admit_weight[..., None, None] * (
        key_vec[..., :, None] * values[..., None, :]
    )
    new_normalizer = keep_weight[..., None] * normalizer + admit_weight[..., None] * key_vec
    numerator = jnp.einsum("bhd,bhdv->bhv", queries, new_memory, precision=lax.Precision.HIGHEST)
    denominator = jnp.sum(queries * new_normalizer, axis=-1)
    cell_out = numerator / jnp.maximum(jnp.abs(denominator), jnp.exp(-new_max))[..., None]
    head_mean = jnp.mean(cell_out, axis=-1, keepdims=True)
    centered = cell_out - head_mean
    head_var = jnp.mean(centered * centered, axis=-1, keepdims=True)
    mixed = (
        (jax.nn.sigmoid(outgate) * centered * lax.rsqrt(head_var + 1e-05))
        .reshape(local_rows, head_count * head_dim)
        .astype(jnp.bfloat16)
    )
    branch_out = jnp.dot(
        lax.all_gather(mixed, "tp", axis=1, tiled=True),
        w_output,
        preferred_element_type=jnp.float32,
    )
    resid = (tokens.astype(jnp.float32) + branch_out).astype(jnp.bfloat16)
    every_row = lax.all_gather(resid, "kv", axis=0, tiled=True)
    every_f = every_row.astype(jnp.float32)
    square_part = jnp.sum(every_f * every_f, axis=-1)
    ffn_in = (every_f * ffn_gain).astype(jnp.bfloat16)
    gate_part = jnp.dot(ffn_in, w_gate, preferred_element_type=jnp.float32)
    up_part = jnp.dot(ffn_in, w_up, preferred_element_type=jnp.float32)
    gate_full, up_full, square_full = (
        lax.psum(gate_part.astype(jnp.bfloat16), "tp").astype(jnp.float32),
        lax.psum(up_part.astype(jnp.bfloat16), "tp").astype(jnp.float32),
        lax.psum(square_part.astype(jnp.bfloat16), "tp").astype(jnp.float32),
    )
    hidden = activate(gate_full, up_full, square_full)
    down_out = lax.psum_scatter(
        jnp.dot(hidden, w_down, preferred_element_type=jnp.float32),
        "kv",
        scatter_dimension=0,
        tiled=True,
    )
    result = (resid.astype(jnp.float32) + down_out).astype(jnp.bfloat16)
    return (result, new_memory, new_normalizer, new_max)


def solution(mesh):
    placed = (
        P("kv", "tp"),
        P(),
        P(None, "tp"),
        P(None, "tp"),
        P(None, "tp"),
        P(None, "tp"),
        P(),
        P(),
        P("kv", "tp", None, None),
        P("kv", "tp", None),
        P("kv", "tp"),
        P(None, "tp"),
        P("tp"),
        P("tp", "kv"),
        P("tp", "kv"),
        P("kv", "tp"),
    )
    return jax.shard_map(
        per_device,
        mesh=mesh,
        in_specs=placed,
        out_specs=(P("kv", "tp"), P("kv", "tp", None, None), P("kv", "tp", None), P("kv", "tp")),
        check_vma=False,
    )
```

profile of v0, /device:TPU:0, one launch (start us, length us, event | category | flops | bytes accessed | tf_op | source)
XLA Modules:
  0.0 181.3 jit_solution(10911743880774895137)
XLA Ops:
  7.2 0.0 all-reduce.3.cloned.1.call-start
  7.3 2.3 %all_gather.9 = bf16[16,2048]{1,0:T(8,128)(2,1)S(1)} all-gather(bf16[16,1024]{1,0:T(8,128)(2,1)} %param.16), channel_id=1, replica_groups=mesh['kv'=16,'tp'=2] {'tp'}, dimensions={1}, use_global_device_ids=true | all-gather | bytes 98304 | tf_op jit(solution)/shard_map/all_gather | solution.py:35
  9.6 0.1 fusion.11
  9.8 2.0 %convolution_multiply_fusion = f32[16,512]{1,0:T(8,128)S(1)} fusion(bf16[2048,512]{1,0:T(8,128)(2,1)} %param.18, bf16[16,2048]{1,0:T(8,128)(2,1)S(1)} %all_gather.9, f32[2048]{0:T(1024)} %param.17, f32[16]{0:T(128)S(1)} %add_rsqrt_fusion.2), kind=kOutput, calls=%fused_computation.7 | convolution fusion | flops 33693696 | bytes 2203712 | tf_op jit(solution)/shard_map/dot_general | solution.py:41
  11.9 0.2 fusion.21
  12.1 0.2 fusion.23
  12.3 0.1 copy.25
  12.4 0.1 copy.26
  12.5 2.0 %fusion.19 = f32[16,512]{1,0:T(8,128)S(1)} fusion(bf16[2048,512]{1,0:T(8,128)(2,1)} %param.19, bf16[16,2048]{1,0:T(8,128)(2,1)S(1)} %all_gather.9, f32[2048]{0:T(1024)S(1)} %copy-done.3, f32[16]{0:T(128)S(1)} %add_rsqrt_fusion.2), kind=kOutput, calls=%fused_computation.43 | convolution fusion | flops 33685504 | bytes 2203712 | tf_op jit(solution)/shard_map/dot_general | solution.py:41
  14.6 0.7 multiply_reduce_fusion.1
  15.3 0.1 copy.29
  15.4 0.1 copy.30
  15.5 2.2 %fusion.17 = f32[16,512]{1,0:T(8,128)S(1)} fusion(bf16[2048,512]{1,0:T(8,128)(2,1)} %param.20, bf16[16,2048]{1,0:T(8,128)(2,1)S(1)} %all_gather.9, f32[2048]{0:T(1024)S(1)} %copy-done.3, f32[16]{0:T(128)S(1)} %add_rsqrt_fusion.2), kind=kOutput, calls=%fused_computation.42 | convolution fusion | flops 33685504 | bytes 2203712 | tf_op jit(solution)/shard_map/dot_general | solution.py:41
  17.6 0.1 copy-done.2
  17.7 0.4 fusion.3
  18.2 3.7 %multiply_add_fusion = f32[16,4,128,128]{3,2,1,0:T(8,128)S(1)} fusion(f32[16,4,128,128]{3,2,1,0:T(8,128)} %param.24, f32[16,4,128]{2,1,0:T(4,128)S(1)} %mul.143, f32[16,4,128]{2,1,0:T(4,128)S(1)} %mul.141, f32[16,4]{1,0:T(8,128)S(1)} %copy.26, f32[16,4]{1,0:T(8,128)S(1)} %copy.25), kind=kLoop, calls=%fused_computation | loop fusion | flops 4194304 | bytes 8454656 | tf_op jit(solution)/shard_map/add | solution.py:63
  21.9 3.7 %fusion.28 = f32[16,4,1,128]{3,2,1,0:T(1,128)S(1)} fusion(f32[16,4,128,1]{2,3,1,0:T(1,128)S(1)} %bitcast.20, f32[16,4,128,128]{3,2,1,0:T(8,128)S(1)} %multiply_add_fusion), kind=kOutput, calls=%fused_computation.47 | convolution fusion | flops 12582912 | bytes 4259840 | tf_op jit(solution)/shard_map/bhd,bhdv->bhv/dot_general | solution.py:67
  25.6 0.2 fusion.27
  25.8 0.2 multiply_reduce_fusion
  26.0 0.1 multiply_convert_fusion.2
  26.1 1.8 %all_gather.10 = bf16[16,1024]{1,0:T(8,128)(2,1)S(1)} all-gather(bf16[16,512]{1,0:T(8,128)(2,1)S(1)} %bitcast.22), channel_id=1, replica_groups=mesh['kv'=16,'tp'=2] {'tp'}, dimensions={1}, use_global_device_ids=true | all-gather | bytes 49152 | tf_op jit(solution)/shard_map/all_gather | solution.py:79
  27.9 0.4 fusion
  28.3 45.4 %all_gather.11 = bf16[256,1024]{1,0:T(8,128)(2,1)S(1)} all-gather(bf16[16,1024]{1,0:T(8,128)(2,1)S(1)} %fusion), channel_id=1, replica_groups=mesh['kv'=16,'tp'=2] {'kv'}, dimensions={0}, use_global_device_ids=true | all-gather | bytes 557056 | tf_op jit(solution)/shard_map/all_gather | solution.py:84
  73.7 1.1 convolution_convert_fusion
  74.8 1.1 convolution_convert_fusion.1
  75.9 0.0 reduce-scatter.2.cloned.1.call-start
  75.9 0.2 fusion.4
  76.1 2.5 %psum.21 = bf16[256]{0:T(256)(128)(2,1)S(1)} all-reduce(bf16[256]{0:T(256)(128)(2,1)S(1)} %fusion.4), channel_id=1, replica_groups=mesh['kv'=16,'tp'=2] {'tp'}, use_global_device_ids=true, to_apply=%region_5.6 | all-reduce | flops 256 | bytes 1024 | tf_op jit(solution)/shard_map/psum | solution.py:93
  78.6 11.7 %all-reduce.3.cloned.1.call-done = (bf16[256,352]{0,1:T(8,128)(2,1)}, bf16[256,352]{0,1:T(8,128)(2,1)}) async-done(((bf16[256,352]{0,1:T(8,128)(2,1)}, bf16[256,352]{0,1:T(8,128)(2,1)}), (bf16[256,352]{0,1:T(8,128)(2,1)}, bf16[256,352]{0,1:T(8,128)(2,1)})) %all-reduce.3.cloned.1.call-update) | async-done | bytes 360464 | tf_op jit(solution)/shard_map/psum | solution.py:92
  90.3 2.5 %fusion.8 = f32[256,1024]{1,0:T(8,128)} fusion(bf16[352,1024]{1,0:T(8,128)(2,1)S(1)} %copy-done.10, bf16[256,352]{0,1:T(8,128)(2,1)} %get-tuple-element.4, bf16[256,352]{0,1:T(8,128)(2,1)} %get-tuple-element.5, f32[256]{0:T(256)S(1)} %add_rsqrt_fusion.1), kind=kOutput, calls=%fused_computation.15 | convolution fusion | flops 185450496 | bytes 2130944 | tf_op jit(solution)/shard_map/dot_general | solution.py:97
  92.9 80.1 %reduce-scatter.2.cloned.1.call-done = f32[16,1024]{1,0:T(8,128)} async-done(((f32[256,1024]{1,0:T(8,128)}), f32[16,1024]{1,0:T(8,128)}) %reduce-scatter.2.cloned.1.call-update) | async-done | bytes 65552 | tf_op jit(solution)/shard_map/reduce_scatter | solution.py:96
  173.0 1.5 add_convert_fusion
  (42 shorter events, 0.3 us)
Async XLA Ops:
  7.2 20.7 %copy-start = (bf16[1024,1024]{1,0:T(8,128)(2,1)S(1)}, bf16[1024,1024]{1,0:T(8,128)(2,1)}, u32[]{:S(2)}) copy-start(bf16[1024,1024]{1,0:T(8,128)(2,1)} %param.27) | copy-start | bytes 6291460
  7.2 4.7 %copy-start.3 = (f32[2048]{0:T(1024)S(1)}, f32[2048]{0:T(1024)}, u32[]{:S(2)}) copy-start(f32[2048]{0:T(1024)} %param.17) | copy-start | bytes 24580
  7.2 4.7 %copy-start.11 = (bf16[2048,8]{0,1:T(8,128)(2,1)S(1)}, bf16[2048,8]{0,1:T(8,128)(2,1)}, u32[]{:S(2)}) copy-start(bf16[2048,8]{0,1:T(8,128)(2,1)} %param.22) | copy-start | bytes 98308
  7.2 4.9 %copy-start.12 = (bf16[2048,8]{0,1:T(8,128)(2,1)S(1)}, bf16[2048,8]{0,1:T(8,128)(2,1)}, u32[]{:S(2)}) copy-start(bf16[2048,8]{0,1:T(8,128)(2,1)} %param.23) | copy-start | bytes 98308
  7.2 5.1 %copy-start.7 = (f32[16,4]{0,1:T(4,128)S(1)}, f32[16,4]{0,1:T(4,128)}, u32[]{:S(2)}) copy-start(f32[16,4]{0,1:T(4,128)} %param.26) | copy-start | bytes 772
  7.2 83.1 %all-reduce.3.cloned.1.call-start = ((), (), s32[]{:S(2)}) async-start(), calls=%async_computation.2 | async-start | bytes 720896 | tf_op jit(solution)/shard_map/psum | solution.py:92
  9.8 4.8 %copy-start.5 = (f32[16,4,128]{2,1,0:T(4,128)S(1)}, f32[16,4,128]{2,1,0:T(4,128)}, u32[]{:S(2)}) copy-start(f32[16,4,128]{2,1,0:T(4,128)} %param.25) | copy-start | bytes 98308
  12.3 5.3 %copy-start.6 = (f32[16,4]{0,1:T(4,128)}, f32[16,4]{0,1:T(4,128)S(1)}, u32[]{:S(2)}) copy-start(f32[16,4]{0,1:T(4,128)S(1)} %get-tuple-element.11) | copy-start | bytes 772
  15.4 2.2 %copy-start.2 = (bf16[2048,512]{1,0:T(8,128)(2,1)S(1)}, bf16[2048,512]{1,0:T(8,128)(2,1)}, u32[]{:S(2)}) copy-start(bf16[2048,512]{1,0:T(8,128)(2,1)} %param.21) | copy-start | bytes 6291460
  21.9 3.7 %copy-start.1 = (f32[16,4,128,128]{3,2,1,0:T(8,128)}, f32[16,4,128,128]{3,2,1,0:T(8,128)S(1)}, u32[]{:S(2)}) copy-start(f32[16,4,128,128]{3,2,1,0:T(8,128)S(1)} %multiply_add_fusion) | copy-start | bytes 12582916
  21.9 6.0 %copy-start.4 = (bf16[16,1024]{1,0:T(8,128)(2,1)S(1)}, bf16[16,1024]{1,0:T(8,128)(2,1)}, u32[]{:S(2)}) copy-start(bf16[16,1024]{1,0:T(8,128)(2,1)} %param.16) | copy-start | bytes 98308
  25.6 48.1 %copy-start.8 = (bf16[1024,352]{0,1:T(8,128)(2,1)S(1)}, bf16[1024,352]{0,1:T(8,128)(2,1)}, u32[]{:S(2)}) copy-start(bf16[1024,352]{0,1:T(8,128)(2,1)} %param.30) | copy-start | bytes 2162692
  25.6 48.1 %copy-start.13 = (f32[1024]{0:T(1024)S(1)}, f32[1024]{0:T(1024)}, u32[]{:S(2)}) copy-start(f32[1024]{0:T(1024)} %param.28) | copy-start | bytes 12292
  27.9 46.9 %copy-start.9 = (bf16[1024,352]{0,1:T(8,128)(2,1)S(1)}, bf16[1024,352]{0,1:T(8,128)(2,1)}, u32[]{:S(2)}) copy-start(bf16[1024,352]{0,1:T(8,128)(2,1)} %param.29) | copy-start | bytes 2162692
  73.7 16.6 %copy-start.10 = (bf16[352,1024]{1,0:T(8,128)(2,1)S(1)}, bf16[352,1024]{1,0:T(8,128)(2,1)}, u32[]{:S(2)}) copy-start(bf16[352,1024]{1,0:T(8,128)(2,1)} %param.31) | copy-start | bytes 2162692
  75.9 97.1 %reduce-scatter.2.cloned.1.call-start = ((), (), s32[]{:S(2)}) async-start(), calls=%async_computation.1 | async-start | bytes 1114112 | tf_op jit(solution)/shard_map/reduce_scatter | solution.py:96
Sparse Core Ops, SparseCore 0:
  76.0 14.2 all-reduce.2
  93.0 79.9 reduce-scatter.1
where the time goes:
time: 182 us; the launch traced here: 181 us
  waiting for transfers between devices  91.8 us (50%)
  blocking collectives  52 us (29%)
  matrix products  15.8 us (9%)
  between operations  14.3 us (8%)
  other arithmetic  6.72 us (4%)
    reduce_scatter x1, waiting for transfers between devices, per_device(): lax.psum_scatter(jnp.dot(hidden, w_down, preferred_element_type=jnp.float...  80.1 us
    all_gather x1, blocking collectives, per_device(): every_row = lax.all_gather(resid, 'kv', axis=0, tiled=True)  45.4 us
    psum x1, waiting for transfers between devices, per_device(): lax.psum(up_part.astype(jnp.bfloat16), 'tp').astype(jnp.float32)  11.7 us
    dot_general x4, matrix products, project(): jnp.dot(normed, weight, preferred_element_type=jnp.float32)  6.65 us
    add x1, other arithmetic, per_device(): keep_weight[..., None, None] * memory  3.72 us
    dot_general x1, matrix products, per_device(): jnp.einsum('bhd,bhdv->bhv', queries, new_memory, precision=lax.Precision....  3.66 us
  transfers between devices with their start and end apart: 2, of which 2 were waited for; matrix products, arithmetic and copies ran while one was open for 0% of the time, Pallas kernels for 0%

commit v1 on v0

--- a/solution.py
+++ b/solution.py
@@ -81,7 +81,8 @@
         preferred_element_type=jnp.float32,
     )
     resid = (tokens.astype(jnp.float32) + branch_out).astype(jnp.bfloat16)
-    every_row = lax.all_gather(resid, "kv", axis=0, tiled=True)
+    outgoing = jnp.stack([resid] * lax.axis_size("kv"))
+    every_row = jnp.concatenate(lax.all_to_all(outgoing, "kv", 0, 0), axis=0)
     every_f = every_row.astype(jnp.float32)
     square_part = jnp.sum(every_f * every_f, axis=-1)
     ffn_in = (every_f * ffn_gain).astype(jnp.bfloat16)

time: 182 us -> 163 us (0.90)
  blocking collectives: 52 us -> 30.2 us
  waiting for transfers between devices: 91.8 us -> 94.3 us
    all_gather x1 -> x0, blocking collectives: 45.4 us -> none  [per_device(): every_row = lax.all_gather(resid, 'kv', axis=0, tiled=True)]
    all_to_all x0 -> x1, blocking collectives: none -> 23.5 us  [per_device(): every_row = jnp.concatenate(lax.all_to_all(outgoing, 'kv', 0, 0), axis=0)]
    psum x1, waiting for transfers between devices: 11.7 us -> 14.1 us  [per_device(): lax.psum(up_part.astype(jnp.bfloat16), 'tp').astype(jnp.float32)]
where the time goes in v1:
time: 163 us; the launch traced here: 162 us
  waiting for transfers between devices  94.3 us (58%)
  blocking collectives  30.2 us (19%)
  matrix products  15.8 us (10%)
  between operations  14.3 us (9%)
  other arithmetic  6.83 us (4%)
    reduce_scatter x1, waiting for transfers between devices, per_device(): lax.psum_scatter(jnp.dot(hidden, w_down, preferred_element_type=jnp.float...  80.1 us
    all_to_all x1, blocking collectives, per_device(): every_row = jnp.concatenate(lax.all_to_all(outgoing, 'kv', 0, 0), axis=0)  23.5 us
    psum x1, waiting for transfers between devices, per_device(): lax.psum(up_part.astype(jnp.bfloat16), 'tp').astype(jnp.float32)  14.1 us
    dot_general x4, matrix products, project(): jnp.dot(normed, weight, preferred_element_type=jnp.float32)  6.65 us
    add x1, other arithmetic, per_device(): keep_weight[..., None, None] * memory  3.72 us
    dot_general x1, matrix products, per_device(): jnp.einsum('bhd,bhdv->bhv', queries, new_memory, precision=lax.Precision....  3.66 us
  transfers between devices with their start and end apart: 2, of which 2 were waited for; matrix products, arithmetic and copies ran while one was open for 0% of the time, Pallas kernels for 0%

profile of v1, /device:TPU:0, one launch (start us, length us, event | category | flops | bytes accessed | tf_op | source)
XLA Modules:
  0.0 162.1 jit_solution(9474226026971016227)
XLA Ops:
  7.3 2.3 %all_gather.6 = bf16[16,2048]{1,0:T(8,128)(2,1)S(1)} all-gather(bf16[16,1024]{1,0:T(8,128)(2,1)} %param.16), channel_id=1, replica_groups=mesh['kv'=16,'tp'=2] {'tp'}, dimensions={1}, use_global_device_ids=true | all-gather | bytes 98304 | tf_op jit(solution)/shard_map/all_gather | solution.py:35
  9.6 0.1 fusion.8
  9.8 2.0 %convolution_multiply_fusion = f32[16,512]{1,0:T(8,128)S(1)} fusion(bf16[2048,512]{1,0:T(8,128)(2,1)} %param.18, bf16[16,2048]{1,0:T(8,128)(2,1)S(1)} %all_gather.6, f32[2048]{0:T(1024)} %param.17, f32[16]{0:T(128)S(1)} %add_rsqrt_fusion.2), kind=kOutput, calls=%fused_computation.5 | convolution fusion | flops 33693696 | bytes 2203712 | tf_op jit(solution)/shard_map/dot_general | solution.py:41
  11.9 0.2 fusion.18
  12.1 0.2 fusion.20
  12.3 0.1 copy.31
  12.4 0.1 copy.32
  12.5 2.0 %fusion.16 = f32[16,512]{1,0:T(8,128)S(1)} fusion(bf16[2048,512]{1,0:T(8,128)(2,1)} %param.19, bf16[16,2048]{1,0:T(8,128)(2,1)S(1)} %all_gather.6, f32[2048]{0:T(1024)S(1)} %copy-done.5, f32[16]{0:T(128)S(1)} %add_rsqrt_fusion.2), kind=kOutput, calls=%fused_computation.42 | convolution fusion | flops 33685504 | bytes 2203712 | tf_op jit(solution)/shard_map/dot_general | solution.py:41
  14.6 0.7 multiply_reduce_fusion.2
  15.3 0.1 copy.35
  15.4 0.1 copy.36
  15.5 2.2 %fusion.14 = f32[16,512]{1,0:T(8,128)S(1)} fusion(bf16[2048,512]{1,0:T(8,128)(2,1)} %param.20, bf16[16,2048]{1,0:T(8,128)(2,1)S(1)} %all_gather.6, f32[2048]{0:T(1024)S(1)} %copy-done.5, f32[16]{0:T(128)S(1)} %add_rsqrt_fusion.2), kind=kOutput, calls=%fused_computation.41 | convolution fusion | flops 33685504 | bytes 2203712 | tf_op jit(solution)/shard_map/dot_general | solution.py:41
  17.6 0.1 copy-done.2
  17.7 0.4 fusion.3
  18.2 3.7 %multiply_add_fusion = f32[16,4,128,128]{3,2,1,0:T(8,128)S(1)} fusion(f32[16,4,128,128]{3,2,1,0:T(8,128)} %param.24, f32[16,4,128]{2,1,0:T(4,128)S(1)} %mul.144, f32[16,4,128]{2,1,0:T(4,128)S(1)} %mul.142, f32[16,4]{1,0:T(8,128)S(1)} %copy.32, f32[16,4]{1,0:T(8,128)S(1)} %copy.31), kind=kLoop, calls=%fused_computation | loop fusion | flops 4194304 | bytes 8454656 | tf_op jit(solution)/shard_map/add | solution.py:63
  21.9 3.7 %fusion.25 = f32[16,4,1,128]{3,2,1,0:T(1,128)S(1)} fusion(f32[16,4,128,1]{2,3,1,0:T(1,128)S(1)} %bitcast.26, f32[16,4,128,128]{3,2,1,0:T(8,128)S(1)} %multiply_add_fusion), kind=kOutput, calls=%fused_computation.46 | convolution fusion | flops 12582912 | bytes 4259840 | tf_op jit(solution)/shard_map/bhd,bhdv->bhv/dot_general | solution.py:67
  25.6 0.2 fusion.24
  25.8 0.2 multiply_reduce_fusion.1
  26.0 0.1 multiply_convert_fusion.2
  26.1 1.8 %all_gather.7 = bf16[16,1024]{1,0:T(8,128)(2,1)S(1)} all-gather(bf16[16,512]{1,0:T(8,128)(2,1)S(1)} %bitcast.28), channel_id=1, replica_groups=mesh['kv'=16,'tp'=2] {'tp'}, dimensions={1}, use_global_device_ids=true | all-gather | bytes 49152 | tf_op jit(solution)/shard_map/all_gather | solution.py:79
  27.9 0.4 fusion
  28.4 23.5 %all_to_all.5 = bf16[16,16,1024]{2,1,0:T(8,128)(2,1)S(1)} all-to-all(bf16[16,16,1024]{2,1,0:T(8,128)(2,1)S(1)} %stack.2), channel_id=1, replica_groups=mesh['kv'=16,'tp'=2] {'kv'}, dimensions={0} | all-to-all | bytes 1048576 | tf_op jit(solution)/shard_map/all_to_all | solution.py:85
  51.9 0.1 fusion.4
  52.1 1.1 convolution_convert_fusion
  53.1 1.1 convolution_convert_fusion.1
  54.3 0.2 multiply_reduce_fusion
  54.4 0.1 convert_element_type.69
  54.5 2.5 %psum.21 = bf16[256]{0:T(256)(128)(2,1)S(1)} all-reduce(bf16[256]{0:T(256)(128)(2,1)S(1)} %convert_element_type.69), channel_id=1, replica_groups=mesh['kv'=16,'tp'=2] {'tp'}, use_global_device_ids=true, to_apply=%region_5.6 | all-reduce | flops 256 | bytes 1024 | tf_op jit(solution)/shard_map/psum | solution.py:94
  57.0 14.1 %all-reduce.3.cloned.1.call-done = (bf16[256,352]{0,1:T(8,128)(2,1)}, bf16[256,352]{0,1:T(8,128)(2,1)}) async-done(((bf16[256,352]{0,1:T(8,128)(2,1)}, bf16[256,352]{0,1:T(8,128)(2,1)}), (bf16[256,352]{0,1:T(8,128)(2,1)}, bf16[256,352]{0,1:T(8,128)(2,1)})) %all-reduce.3.cloned.1.call-update) | async-done | bytes 360464 | tf_op jit(solution)/shard_map/psum | solution.py:93
  71.1 2.5 %fusion.5 = f32[256,1024]{1,0:T(8,128)} fusion(bf16[352,1024]{1,0:T(8,128)(2,1)S(1)} %copy-done.11, bf16[256,352]{0,1:T(8,128)(2,1)} %get-tuple-element.4, bf16[256,352]{0,1:T(8,128)(2,1)} %get-tuple-element.5, f32[256]{0:T(256)S(1)} %add_rsqrt_fusion.1), kind=kOutput, calls=%fused_computation.14 | convolution fusion | flops 185450496 | bytes 2130944 | tf_op jit(solution)/shard_map/dot_general | solution.py:98
  73.7 80.1 %reduce-scatter.2.cloned.1.call-done = f32[16,1024]{1,0:T(8,128)} async-done(((f32[256,1024]{1,0:T(8,128)}), f32[16,1024]{1,0:T(8,128)}) %reduce-scatter.2.cloned.1.call-update) | async-done | bytes 65552 | tf_op jit(solution)/shard_map/reduce_scatter | solution.py:97
  153.8 1.5 add_convert_fusion
  (45 shorter events, 0.4 us)
Async XLA Ops:
  7.2 20.7 %copy-start = (bf16[1024,1024]{1,0:T(8,128)(2,1)S(1)}, bf16[1024,1024]{1,0:T(8,128)(2,1)}, u32[]{:S(2)}) copy-start(bf16[1024,1024]{1,0:T(8,128)(2,1)} %param.27) | copy-start | bytes 6291460
  7.2 4.7 %copy-start.5 = (f32[2048]{0:T(1024)S(1)}, f32[2048]{0:T(1024)}, u32[]{:S(2)}) copy-start(f32[2048]{0:T(1024)} %param.17) | copy-start | bytes 24580
  7.2 4.7 %copy-start.12 = (bf16[2048,8]{0,1:T(8,128)(2,1)S(1)}, bf16[2048,8]{0,1:T(8,128)(2,1)}, u32[]{:S(2)}) copy-start(bf16[2048,8]{0,1:T(8,128)(2,1)} %param.22) | copy-start | bytes 98308
  7.2 4.9 %copy-start.13 = (bf16[2048,8]{0,1:T(8,128)(2,1)S(1)}, bf16[2048,8]{0,1:T(8,128)(2,1)}, u32[]{:S(2)}) copy-start(bf16[2048,8]{0,1:T(8,128)(2,1)} %param.23) | copy-start | bytes 98308
  7.2 5.1 %copy-start.10 = (f32[16,4]{0,1:T(4,128)S(1)}, f32[16,4]{0,1:T(4,128)}, u32[]{:S(2)}) copy-start(f32[16,4]{0,1:T(4,128)} %param.26) | copy-start | bytes 772
  7.2 63.9 %all-reduce.3.cloned.1.call-start = ((), (), s32[]{:S(2)}) async-start(), calls=%async_computation.3 | async-start | bytes 720896 | tf_op jit(solution)/shard_map/psum | solution.py:93
  9.8 4.8 %copy-start.7 = (f32[16,4,128]{2,1,0:T(4,128)S(1)}, f32[16,4,128]{2,1,0:T(4,128)}, u32[]{:S(2)}) copy-start(f32[16,4,128]{2,1,0:T(4,128)} %param.25) | copy-start | bytes 98308
  12.3 5.3 %copy-start.8 = (f32[16,4]{0,1:T(4,128)}, f32[16,4]{0,1:T(4,128)S(1)}, u32[]{:S(2)}) copy-start(f32[16,4]{0,1:T(4,128)S(1)} %get-tuple-element.11) | copy-start | bytes 772
  15.4 2.2 %copy-start.2 = (bf16[2048,512]{1,0:T(8,128)(2,1)S(1)}, bf16[2048,512]{1,0:T(8,128)(2,1)}, u32[]{:S(2)}) copy-start(bf16[2048,512]{1,0:T(8,128)(2,1)} %param.21) | copy-start | bytes 6291460
  21.9 3.7 %copy-start.1 = (f32[16,4,128,128]{3,2,1,0:T(8,128)}, f32[16,4,128,128]{3,2,1,0:T(8,128)S(1)}, u32[]{:S(2)}) copy-start(f32[16,4,128,128]{3,2,1,0:T(8,128)S(1)} %multiply_add_fusion) | copy-start | bytes 12582916
  21.9 6.0 %copy-start.6 = (bf16[16,1024]{1,0:T(8,128)(2,1)S(1)}, bf16[16,1024]{1,0:T(8,128)(2,1)}, u32[]{:S(2)}) copy-start(bf16[16,1024]{1,0:T(8,128)(2,1)} %param.16) | copy-start | bytes 98308
  25.6 26.3 %copy-start.9 = (f32[1024]{0:T(1024)S(1)}, f32[1024]{0:T(1024)}, u32[]{:S(2)}) copy-start(f32[1024]{0:T(1024)} %param.28) | copy-start | bytes 12292
  27.9 24.1 %copy-start.3 = (bf16[1024,352]{0,1:T(8,128)(2,1)S(1)}, bf16[1024,352]{0,1:T(8,128)(2,1)}, u32[]{:S(2)}) copy-start(bf16[1024,352]{0,1:T(8,128)(2,1)} %param.30) | copy-start | bytes 2162692
  28.3 24.8 %copy-start.4 = (bf16[1024,352]{0,1:T(8,128)(2,1)S(1)}, bf16[1024,352]{0,1:T(8,128)(2,1)}, u32[]{:S(2)}) copy-start(bf16[1024,352]{0,1:T(8,128)(2,1)} %param.29) | copy-start | bytes 2162692
  52.0 19.1 %copy-start.11 = (bf16[352,1024]{1,0:T(8,128)(2,1)S(1)}, bf16[352,1024]{1,0:T(8,128)(2,1)}, u32[]{:S(2)}) copy-start(bf16[352,1024]{1,0:T(8,128)(2,1)} %param.31) | copy-start | bytes 2162692
  54.2 99.6 %reduce-scatter.2.cloned.1.call-start = ((), (), s32[]{:S(2)}) async-start(), calls=%async_computation.2 | async-start | bytes 1114112 | tf_op jit(solution)/shard_map/reduce_scatter | solution.py:97
Sparse Core Ops, SparseCore 0:
  54.3 16.7 all-reduce.2
  73.8 79.9 reduce-scatter.1
